TPU v7x, 32 devices: a whole 2x2x4 slice. The times are simulated.
32 devices in a mesh: ep: 4 (over y, x), tp: 8 (over z, core).
Axes of the slice: x: 2, y: 2, z: 4, core: 2. Of those that a mesh axis runs over, the one named last changes fastest.
Arguments:
- queries: bfloat16 [3072, 2048], P('ep', 'tp'), may hold values from -6 to 6
- keys: bfloat16 [3072, 512], P('ep'), may hold values from -6 to 6
- values: bfloat16 [3072, 512], P('ep'), may hold values from -6 to 6
- query_gain: float32 [128], replicated, may hold values from 1 to 4.5
- key_gain: float32 [128], replicated, may hold values from 1 to 4.5
- out_weight: bfloat16 [2048, 2048], P('tp'), may hold values from -0.75 to 0.75
- tokens_b: bfloat16 [1536, 2048], P('ep'), may hold values from -6 to 6
- norm_gain: float32 [2048], replicated, may hold values from 0.1 to 1.9
- routes: int32 [1536, 2], P('ep'), may hold values from 0 to 15, all different within a row; in each aligned block of 48 rows (0 to 47, 48 to 95, ...) at most 8 rows name the same one
- route_weight: float32 [1536, 2], P('ep'), may hold values from 0.2 to 1
- gate_weight: bfloat16 [16, 2048, 4096], P('ep', None, 'tp'), may hold values from -0.125 to 0.125
- up_weight: bfloat16 [16, 2048, 4096], P('ep', None, 'tp'), may hold values from -0.125 to 0.125
- down_weight: bfloat16 [16, 4096, 2048], P('ep', 'tp'), may hold values from -0.09375 to 0.09375
Outputs:
- mixed_out: bfloat16 [3072, 2048], P(('ep', 'tp'))
- expert_out: bfloat16 [1536, 2048], P(('ep', 'tp'))
Inputs may be any that keep to these rules, and one draw needn't show every extreme that they name: `routes`: A row names 2 different experts. In each aligned block of 48 rows no expert is named more than 8 times, a bound that some block reaches.
All inputs are finite; a program needn't handle non-finite values.
Results may differ from a plain program's by a relative error of at most 0.019.
Values may be sent and summed in bfloat16 or wider, within the bound.
A program may use at most 128 MiB of HBM per device.

v0:
```python
import functools

import jax
import jax.numpy as jnp
from jax import lax
from jax.experimental import pallas as pl
from jax.experimental.pallas import tpu as pltpu
from jax.sharding import PartitionSpec as P

HD = 128
HQ = 16
KVH = 4
EXPERTS = 16
TOPK = 2
GRID_W = 64
CAP = 8
EPS = 1e-06
THETA = 10000.0
LOG2E = 1.4426950408889634
MESH = pl.DeviceIdType.MESH
BF = jnp.bfloat16
F32 = jnp.float32


def remote(src, dst, send, recv, device):
    return pltpu.make_async_remote_copy(
        src_ref=src,
        dst_ref=dst,
        send_sem=send,
        recv_sem=recv,
        device_id=device,
        device_id_type=MESH,
    )


def turned(x, gain, cosine, sine):
    x = x.astype(F32)
    x = x * lax.rsqrt(jnp.mean(x * x, axis=-1, keepdims=True) + EPS) * gain
    lane = lax.broadcasted_iota(jnp.int32, x.shape, 1)
    partner = jnp.where(lane % 64 < 32, pltpu.roll(x, HD - 32, 1), pltpu.roll(x, 32, 1))
    return (x * cosine + partner * sine).astype(BF)


def kernel(
    n_ep,
    n_tp,
    tq,
    q_ref,
    k_ref,
    v_ref,
    cos_ref,
    sin_ref,
    qg_ref,
    kg_ref,
    wo_ref,
    tok_ref,
    ng_ref,
    route_ref,
    share_ref,
    wg_hbm,
    wu_hbm,
    wd_hbm,
    mixed_ref,
    expert_ref,
    wg,
    wu,
    wd,
    kv,
    qn,
    att,
    apart,
    asib,
    azr,
    outb,
    arr,
    both,
    hid,
    part,
    sib,
    ret,
    zs,
    zr,
    w_sem,
    kv_s,
    kv_r,
    kvf_s,
    kvf_r,
    d_s,
    d_r,
    df_s,
    df_r,
    do_s,
    do_r,
    a_s,
    a_r,
    az_s,
    az_r,
    p_s,
    p_r,
    r_s,
    r_r,
    z_s,
    z_r,
):
    ep = lax.axis_index("ep")
    tp = lax.axis_index("tp")
    core = lax.rem(tp, 2)
    z = tp // 2
    n_z = n_tp // 2
    other = 1 - core
    sibling = (ep, z * 2 + other)
    ep_peers = [lax.rem(ep + k, n_ep) for k in range(1, n_ep)]
    z_peers = [lax.rem(z + k, n_z) for k in range(1, n_z)]
    n_rows = k_ref.shape[0]
    heads = q_ref.shape[1] // HD
    depth = tok_ref.shape[1]
    n_local = wg.shape[0]
    slots = n_z * CAP
    block = tok_ref.shape[0] // n_tp
    out_rows = mixed_ref.shape[0]

    weights = []
    for i in range(n_local):
        for j, (src, dst) in enumerate(((wg_hbm, wg), (wu_hbm, wu), (wd_hbm, wd))):
            copy = pltpu.make_async_copy(src.at[i], dst.at[i], w_sem.at[j, i])
            copy.start()
            weights.append(copy)

    barrier = pltpu.get_barrier_semaphore()
    for device in [sibling] + [(p, tp) for p in ep_peers] + [(ep, w * 2 + core) for w in z_peers]:
        pl.semaphore_signal(barrier, inc=1, device_id=device, device_id_type=MESH)

    cosine, sine = cos_ref[...], sin_ref[...]
    kv[0, ep] = turned(k_ref[...], kg_ref[...], cosine, sine)
    kv[1, ep] = v_ref[...]
    pl.semaphore_wait(barrier, n_ep + n_z - 1)
    sends = []
    for p in ep_peers:
        copy = remote(kv.at[core, ep], kv.at[core, ep], kv_s.at[p], kv_r.at[ep], (p, tp))
        copy.start()
        sends.append(copy)

    half = n_z * block
    route = route_ref[...]
    e_iota = lax.broadcasted_iota(jnp.int32, (EXPERTS, half), 0)
    hot0 = (e_iota == route[0:1]).astype(F32)
    hot1 = (e_iota == route[1:2]).astype(F32)
    before = lax.broadcasted_iota(jnp.int32, (half, half), 0)
    after = lax.broadcasted_iota(jnp.int32, (half, half), 1)
    earlier = ((before < after) & (before // block == after // block)).astype(F32)
    count = jnp.dot(
        (hot0 + hot1).astype(BF), earlier.astype(BF), preferred_element_type=F32
    )
    rank0 = jnp.sum(hot0 * count, axis=0, keepdims=True).astype(jnp.int32)
    rank1 = jnp.sum(hot1 * count, axis=0, keepdims=True).astype(jnp.int32)
    base = lax.broadcasted_iota(jnp.int32, (1, half), 1) // block * CAP
    slot0 = route[0:1] * slots + base + rank0
    slot1 = route[1:2] * slots + base + rank1
    j_iota = lax.broadcasted_iota(jnp.int32, (EXPERTS * slots, half), 0)
    is0 = j_iota == slot0
    is1 = j_iota == slot1
    mat = (is0 | is1).astype(F32).astype(BF)
    field = jnp.concatenate(
        [
            tok_ref[pl.ds(pl.multiple_of((2 * w + core) * block, 16), block), :]
            for w in range(n_z)
        ],
        axis=0,
    ).astype(F32)
    normed = (
        field * lax.rsqrt(jnp.mean(field * field, axis=-1, keepdims=True) + EPS) * ng_ref[...]
    ).astype(BF)
    outb[...] = (
        jnp.dot(mat, normed, preferred_element_type=F32)
        .astype(BF)
        .reshape(n_ep, n_local, slots, depth)
    )
    for i in range(n_local):
        for p in ep_peers:
            copy = remote(
                outb.at[p, i], arr.at[i, core, ep], d_s.at[i, p], d_r.at[i, ep], (p, tp)
            )
            copy.start()
            sends.append(copy)
    arr[:, core, ep] = outb[ep]
    copy = remote(outb.at[ep], arr.at[:, core, ep], do_s, do_r, sibling)
    copy.start()
    sends.append(copy)

    for g in range(heads):
        qn[pl.ds(g * n_rows, n_rows), :] = turned(
            q_ref[:, g * HD : (g + 1) * HD], qg_ref[...], cosine, sine
        )

    for p in ep_peers:
        remote(kv.at[core, p], kv.at[core, p], kv_s.at[p], kv_r.at[p], (p, tp)).wait_recv()
        copy = remote(kv.at[core, p], kv.at[core, p], kvf_s.at[p], kvf_r.at[p], sibling)
        copy.start()
        sends.append(copy)
    for p in ep_peers:
        remote(kv.at[other, p], kv.at[other, p], kvf_s.at[p], kvf_r.at[p], sibling).wait_recv()

    share = share_ref[...]
    share = share / jnp.sum(share, axis=0, keepdims=True)
    comb = jnp.where(is0, share[0:1], 0.0) + jnp.where(is1, share[1:2], 0.0)
    high = comb.astype(BF)
    low = (comb - high.astype(F32)).astype(BF)
    both[...] = jnp.concatenate([high, low], axis=1)

    factor = HD ** (-0.5) * LOG2E
    length = n_ep * n_rows

    def attend(i, carry):
        at = pl.multiple_of(i * tq, 16)
        scores = lax.dot_general(
            qn[pl.ds(at, tq), :],
            kv[0].reshape(length, HD),
            (((1,), (1,)), ((), ())),
            preferred_element_type=F32,
        )
        top = jnp.max(scores, axis=1, keepdims=True)
        weight = jnp.exp2((scores - top) * factor)
        total = jnp.sum(weight, axis=1, keepdims=True)
        merged = jnp.dot(
            weight.astype(BF), kv[1].reshape(length, HD), preferred_element_type=F32
        )
        att[pl.ds(at, tq), :] = (merged / total).astype(BF)
        return carry

    def projected(t):
        total = None
        for g in range(heads):
            piece = jnp.dot(
                att[pl.ds(pl.multiple_of(g * n_rows + t * out_rows, 16), out_rows), :],
                wo_ref[pl.ds(g * HD, HD), :],
                preferred_element_type=F32,
            )
            total = piece if total is None else total + piece
        return total

    def hand_over(w):
        own = projected(2 * w + core)
        remote(apart.at[w], asib.at[w], a_s.at[w], a_r.at[w], sibling).wait_recv()
        asib[w] = (own + asib[w].astype(F32)).astype(BF)

    def push(w):
        hand_over(w)
        copy = remote(asib.at[w], azr.at[z], az_s.at[w], az_r.at[z], (ep, w * 2 + core))
        copy.start()
        sends.append(copy)

    chunk = 2 * out_rows // tq
    order = z_peers + [z]
    for k, w in enumerate(order):
        for g in range(heads):
            first = (g * n_rows + w * 2 * out_rows) // tq
            lax.fori_loop(first, first + chunk, attend, 0)
        apart[w] = projected(2 * w + other).astype(BF)
        copy = remote(apart.at[w], asib.at[w], a_s.at[w], a_r.at[w], sibling)
        copy.start()
        sends.append(copy)
        if k > 0:
            push(order[k - 1])
    hand_over(z)

    def pass_on(i):
        for p in ep_peers:
            remote(
                outb.at[p, i], arr.at[i, core, p], d_s.at[i, p], d_r.at[i, p], (p, tp)
            ).wait_recv()
            copy = remote(
                arr.at[i, core, p], arr.at[i, core, p], df_s.at[i, p], df_r.at[i, p], sibling
            )
            copy.start()
            sends.append(copy)

    pass_on(0)
    remote(outb.at[ep], arr.at[:, other, ep], do_s, do_r, sibling).wait_recv()
    for i in range(n_local):
        for copy in weights[3 * i : 3 * i + 3]:
            copy.wait()
        for p in ep_peers:
            remote(
                arr.at[i, other, p], arr.at[i, other, p], df_s.at[i, p], df_r.at[i, p], sibling
            ).wait_recv()
        if i + 1 < n_local:
            pass_on(i + 1)
        x = arr[i].reshape(2 * n_ep * slots, depth)
        gate = jnp.dot(x, wg[i], preferred_element_type=F32)
        up = jnp.dot(x, wu[i], preferred_element_type=F32)
        hid[i] = (gate / (1.0 + jnp.exp(-gate)) * up).astype(BF)

    n_cut, width = part.shape[0], part.shape[-1]

    def give_back(j):
        remote(part.at[j, :, other], sib.at[j], p_s.at[j], p_r.at[j], sibling).wait_recv()
        sib[j] = (part[j, :, core].astype(F32) + sib[j].astype(F32)).astype(BF)
        for p in ep_peers:
            copy = remote(sib.at[j, :, p], ret.at[j, ep], r_s.at[j, p], r_r.at[j, ep], (p, tp))
            copy.start()
            sends.append(copy)
        ret[j, ep] = sib[j, :, ep]

    for j in range(n_cut):
        for i in range(n_local):
            part[j, i] = (
                jnp.dot(
                    hid[i], wd[i, :, j * width : (j + 1) * width], preferred_element_type=F32
                )
                .astype(BF)
                .reshape(2, n_ep, slots, width)
            )
        copy = remote(part.at[j, :, other], sib.at[j], p_s.at[j], p_r.at[j], sibling)
        copy.start()
        sends.append(copy)
        if j > 0:
            give_back(j - 1)
    give_back(n_cut - 1)

    for j in range(n_cut):
        for p in ep_peers:
            remote(
                sib.at[j, :, p], ret.at[j, p], r_s.at[j, p], r_r.at[j, p], (p, tp)
            ).wait_recv()
        rows = lax.dot_general(
            both[...],
            ret[j].reshape(EXPERTS * slots, width),
            (((0,), (0,)), ((), ())),
            preferred_element_type=F32,
        )
        rows = rows[:half] + rows[half:]
        zs[j] = rows.astype(BF).reshape(n_z, block, width)
        for w in z_peers:
            copy = remote(
                zs.at[j, w], zr.at[j, z], z_s.at[j, w], z_r.at[j, z], (ep, w * 2 + core)
            )
            copy.start()
            sends.append(copy)

    total = asib[z].astype(F32)
    for w in z_peers:
        remote(asib.at[w], azr.at[w], az_s.at[w], az_r.at[w], (ep, w * 2 + core)).wait_recv()
        total = total + azr[w].astype(F32)
    mixed_ref[...] = total.astype(BF)
    for j in range(n_cut):
        total = zs[j, z].astype(F32)
        for w in z_peers:
            remote(
                zs.at[j, w], zr.at[j, w], z_s.at[j, w], z_r.at[j, w], (ep, w * 2 + core)
            ).wait_recv()
            total = total + zr[j, w].astype(F32)
        expert_ref[:, j * width : (j + 1) * width] = total.astype(BF)
    for copy in sends:
        copy.wait_send()


def on_device(
    queries,
    keys,
    values,
    query_gain,
    key_gain,
    out_weight,
    tokens_b,
    norm_gain,
    routes,
    route_weight,
    gate_weight,
    up_weight,
    down_weight,
):
    n_ep, n_tp = lax.axis_size("ep"), lax.axis_size("tp")
    ep, tp = lax.axis_index("ep"), lax.axis_index("tp")
    n_z = n_tp // 2
    n_rows = queries.shape[0]
    heads = queries.shape[1] // HD
    depth = tokens_b.shape[1]
    local_rows = tokens_b.shape[0]
    block = local_rows // n_tp
    n_local, _, ff = gate_weight.shape
    slots = n_z * CAP
    length = n_rows * n_ep
    n_cut = 4
    width = depth // n_cut
    tq = 2 * (n_rows // n_tp)
    while tq * length > 256 * 3072:
        tq //= 2

    positions = ep * n_rows + jnp.arange(n_rows, dtype=jnp.int32)
    lane = jnp.arange(HD, dtype=jnp.int32)
    n_freq = HD // 4
    inverse = THETA ** (-(lane % n_freq).astype(F32) / n_freq)
    along = jnp.where(lane[None] < HD // 2, positions[:, None] // GRID_W, positions[:, None] % GRID_W)
    angle = along.astype(F32) * inverse
    cosine = jnp.cos(angle)
    sine = jnp.sin(angle) * jnp.where(lane % (2 * n_freq) < n_freq, -1.0, 1.0)

    kv_index = tp * heads // (HQ // KVH)
    own_keys = lax.dynamic_slice_in_dim(keys, kv_index * HD, HD, 1)
    own_values = lax.dynamic_slice_in_dim(values, kv_index * HD, HD, 1)

    def mine(table):
        split = table.reshape(n_z, 2, block, TOPK)
        own = lax.dynamic_index_in_dim(split, lax.rem(tp, 2), 1, keepdims=False)
        return own.reshape(n_z * block, TOPK).T

    vmem = pl.BlockSpec(memory_space=pltpu.VMEM)
    hbm = pl.BlockSpec(memory_space=pl.ANY)
    dma = pltpu.SemaphoreType.DMA
    out_rows = n_rows // n_tp
    scratch = [
        pltpu.VMEM(gate_weight.shape, BF),
        pltpu.VMEM(up_weight.shape, BF),
        pltpu.VMEM(down_weight.shape, BF),
        pltpu.VMEM((2, n_ep, n_rows, HD), BF),
        pltpu.VMEM((heads * n_rows, HD), BF),
        pltpu.VMEM((heads * n_rows, HD), BF),
        pltpu.VMEM((n_z, out_rows, depth), BF),
        pltpu.VMEM((n_z, out_rows, depth), BF),
        pltpu.VMEM((n_z, out_rows, depth), BF),
        pltpu.VMEM((n_ep, n_local, slots, depth), BF),
        pltpu.VMEM((n_local, 2, n_ep, slots, depth), BF),
        pltpu.VMEM((EXPERTS * slots, 2 * n_z * block), BF),
        pltpu.VMEM((n_local, 2 * n_ep * slots, ff), BF),
        pltpu.VMEM((n_cut, n_local, 2, n_ep, slots, width), BF),
        pltpu.VMEM((n_cut, n_local, n_ep, slots, width), BF),
        pltpu.VMEM((n_cut, n_ep, n_local, slots, width), BF),
        pltpu.VMEM((n_cut, n_z, block, width), BF),
        pltpu.VMEM((n_cut, n_z, block, width), BF),
        dma((3, n_local)),
        dma((n_ep,)),
        dma((n_ep,)),
        dma((n_ep,)),
        dma((n_ep,)),
        dma((n_local, n_ep)),
        dma((n_local, n_ep)),
        dma((n_local, n_ep)),
        dma((n_local, n_ep)),
        dma,
        dma,
        dma((n_z,)),
        dma((n_z,)),
        dma((n_z,)),
        dma((n_z,)),
        dma((n_cut,)),
        dma((n_cut,)),
        dma((n_cut, n_ep)),
        dma((n_cut, n_ep)),
        dma((n_cut, n_z)),
        dma((n_cut, n_z)),
    ]
    return tuple(
        pl.pallas_call(
            functools.partial(kernel, n_ep, n_tp, tq),
            out_shape=(
                jax.ShapeDtypeStruct((out_rows, out_weight.shape[1]), BF),
                jax.ShapeDtypeStruct((block, depth), BF),
            ),
            in_specs=[vmem] * 12 + [hbm] * 3,
            out_specs=(vmem, vmem),
            scratch_shapes=scratch,
            compiler_params=pltpu.CompilerParams(
                collective_id=0, has_side_effects=True, vmem_limit_bytes=67043328
            ),
        )(
            queries,
            own_keys,
            own_values,
            cosine,
            sine,
            query_gain[None],
            key_gain[None],
            out_weight,
            tokens_b,
            norm_gain[None],
            mine(routes),
            mine(route_weight),
            gate_weight,
            up_weight,
            down_weight,
        )
    )


def solution(mesh):
    placed = (
        P("ep", "tp"),
        P("ep", None),
        P("ep", None),
        P(),
        P(),
        P("tp", None),
        P("ep", None),
        P(),
        P("ep", None),
        P("ep", None),
        P("ep", None, "tp"),
        P("ep", None, "tp"),
        P("ep", "tp", None),
    )
    return jax.shard_map(
        on_device,
        mesh=mesh,
        in_specs=placed,
        out_specs=(P(("ep", "tp"), None), P(("ep", "tp"), None)),
        check_vma=False,
    )
```

profile of v0, /device:TPU:0, one launch (start us, length us, event | category | flops | bytes accessed | tf_op | source)
XLA Modules:
  0.0 91.8 jit_solution(7430583804395752487)
XLA Ops:
  0.7 0.8 reshape.103
  1.5 0.7 reshape.104
  2.2 0.8 reshape.105
  3.0 0.7 reshape.106
  3.6 1.8 %constant_dynamic-slice_fusion.2 = (bf16[768,128]{1,0:T(8,128)(2,1)}, bf16[768,128]{1,0:T(8,128)(2,1)}) fusion(bf16[768,512]{1,0:T(8,128)(2,1)} %param.15, s32[]{:T(128)S(6)} %select_n.67, bf16[768,512]{1,0:T(8,128)(2,1)} %param.14), kind=kLoop, calls=%fused_computation.20 | loop fusion | bytes 786436 | tf_op jit(solution)/shard_map/dynamic_slice | solution.py:400
  5.4 2.8 %sine_multiply_fusion = (f32[768,128]{1,0:T(8,128)}, f32[768,128]{1,0:T(8,128)}) fusion(f32[128]{0:T(128)S(1)} %get-tuple-element.4, f32[128]{0:T(128)S(1)} %get-tuple-element.5, s32[768]{0:T(1024)S(1)} %get-tuple-element.8, s32[768]{0:T(1024)S(1)} %get-tuple-element.9, pred[128]{0:T(512)(128)(4,1)S(1)} %iota_compare_fusion), kind=kLoop, calls=%fused_computation | loop fusion | flops 393216 | bytes 793728 | tf_op jit(solution)/shard_map/mul | solution.py:396
  8.2 80.2 %shard_map.140 = (bf16[96,2048]{1,0:T(8,128)(2,1)}, bf16[48,2048]{1,0:T(8,128)(2,1)}) custom-call(bf16[768,256]{1,0:T(8,128)(2,1)} %q_ref.1, bf16[768,128]{1,0:T(8,128)(2,1)} %get-tuple-element.7.k_ref, bf16[768,128]{1,0:T(8,128)(2,1)} %get-tuple-element.6.v_ref, f32[768,128]{1,0:T(8,128)} %get-tuple-element.3.cos_ref, f32[768,128]{1,0:T(8,128)} %get-tuple-element.2.sin_ref, ...), custom_call_target="tpu_custom_call" | custom-call | tf_op jit(solution)/shard_map/pallas_call | solution.py:453
  88.4 1.8 %copy.21 = bf16[96,2048]{1,0:T(8,128)(2,1)} copy(bf16[96,2048]{1,0:T(8,128)(2,1)} %get-tuple-element.12) | data formatting | bytes 786432
  90.2 1.6 %copy.22 = bf16[48,2048]{1,0:T(8,128)(2,1)} copy(bf16[48,2048]{1,0:T(8,128)(2,1)} %get-tuple-element.13) | data formatting | bytes 393216
  (5 shorter events, 0.0 us)
where the time goes:
time: 92.1 us; the launch traced here: 91.8 us
  Pallas kernels  80.2 us (87%)
  local copies, waits for them, and re-layouts  8.08 us (9%)
  other arithmetic  2.83 us (3%)
    pallas_call x1, Pallas kernels, on_device(): pl.pallas_call(functools.partial(kernel, n_ep, n_tp, tq), out_shape=(jax....  80.2 us
    unnamed x2, local copies, waits for them, and re-layouts  3.38 us
    mul x1, other arithmetic, on_device(): sine = jnp.sin(angle) * jnp.where(lane % (2 * n_freq) < n_freq, -1.0, 1.0)  2.8 us

commit v1 on v0

v1 whole, which is shorter than its diff:
```python
import functools

import jax
import jax.numpy as jnp
import numpy as np
from jax import lax
from jax.experimental import pallas as pl
from jax.experimental.pallas import tpu as pltpu
from jax.sharding import PartitionSpec as P

HD = 128
NCUT = 8
HQ = 16
KVH = 4
EXPERTS = 16
TOPK = 2
GRID_W = 64
CAP = 8
EPS = 1e-06
THETA = 10000.0
LOG2E = 1.4426950408889634
MESH = pl.DeviceIdType.MESH
BF = jnp.bfloat16
F32 = jnp.float32


def remote(src, dst, send, recv, device):
    return pltpu.make_async_remote_copy(
        src_ref=src,
        dst_ref=dst,
        send_sem=send,
        recv_sem=recv,
        device_id=device,
        device_id_type=MESH,
    )


def done(ref, sem):
    pltpu.make_async_copy(ref, ref, sem).wait()


def turned(x, gain, cosine, sine):
    x = x.astype(F32)
    x = x * lax.rsqrt(jnp.mean(x * x, axis=-1, keepdims=True) + EPS) * gain
    lane = lax.broadcasted_iota(jnp.int32, x.shape, 1)
    partner = jnp.where(lane % 64 < 32, pltpu.roll(x, HD - 32, 1), pltpu.roll(x, 32, 1))
    return (x * cosine + partner * sine).astype(BF)


def tables(length):
    lane = np.arange(HD)
    n_freq = HD // 4
    inverse = np.float32(THETA) ** (-(lane % n_freq).astype(np.float32) / np.float32(n_freq))
    sign = np.where(lane % (2 * n_freq) < n_freq, -1.0, 1.0)

    def both(count, mine):
        angle = np.arange(count, dtype=np.float32)[:, None] * inverse.astype(np.float32)
        angle = angle.astype(np.float64)
        cosine = np.where(mine, np.cos(angle), 0.0)
        sine = np.where(mine, np.sin(angle) * sign, 0.0)
        return np.stack([cosine, sine]).astype(np.float32)

    return both(length // GRID_W, lane < HD // 2), both(GRID_W, lane >= HD // 2)


def kernel(
    n_ep,
    n_tp,
    q_hbm,
    k_hbm,
    v_hbm,
    row_ref,
    col_ref,
    qg_ref,
    kg_ref,
    wo_hbm,
    tok_hbm,
    ng_ref,
    route_ref,
    share_ref,
    wg_hbm,
    wu_hbm,
    wd_hbm,
    mixed_hbm,
    expert_hbm,
    mixed_ref,
    expert_ref,
    wo,
    trig,
    wg,
    wu,
    wd,
    kv,
    values,
    qn,
    att,
    apart,
    asib,
    azr,
    outb,
    arr,
    both,
    hid,
    part,
    sib,
    ret,
    zs,
    zr,
    in_sem,
    out_sem,
    t_sem,
    w_sem,
    kv_s,
    kv_r,
    kvf_s,
    kvf_r,
    d_s,
    d_r,
    df_s,
    df_r,
    do_s,
    do_r,
    a_s,
    a_r,
    az_s,
    az_r,
    p_s,
    p_r,
    r_s,
    r_r,
    z_s,
    z_r,
):
    ep = lax.axis_index("ep")
    tp = lax.axis_index("tp")
    core = lax.rem(tp, 2)
    z = tp // 2
    n_z = n_tp // 2
    other = 1 - core
    sibling = (ep, z * 2 + other)
    if n_ep == 4:
        peers = [(1, ep + 1 - 2 * lax.rem(ep, 2)), (2, ep + 2 - 4 * (ep // 2)), (3, 3 - ep)]
        back = [0, 1, 2, 3]
        near = 2
    else:
        peers = [(k, lax.rem(ep + k, n_ep)) for k in range(1, n_ep)]
        back = [0] + [n_ep - k for k in range(1, n_ep)]
        near = n_ep - 1
    z_peers = [lax.rem(z + k, n_z) for k in range(1, n_z)]
    n_rows = k_hbm.shape[0]
    heads = q_hbm.shape[1] // HD
    depth = tok_hbm.shape[1]
    n_local = wg.shape[0]
    slots = n_z * CAP
    block = tok_hbm.shape[0] // n_tp
    out_rows = mixed_ref.shape[0]
    half = n_z * block
    pair = 2 * out_rows
    tile = pair
    while tile * n_ep * n_rows > 256 * 3072:
        tile //= 2

    barrier = pltpu.get_barrier_semaphore()
    for device in [sibling] + [(p, tp) for _, p in peers] + [(ep, w * 2 + core) for w in z_peers]:
        pl.semaphore_signal(barrier, inc=1, device_id=device, device_id_type=MESH)

    kv_at = pl.multiple_of(tp * heads // (HQ // KVH) * HD, HD)
    k_raw = values.at[pl.ds(0, n_rows), pl.ds(0, HD)]
    get_k = pltpu.make_async_copy(k_hbm.at[:, pl.ds(kv_at, HD)], k_raw, in_sem.at[0])
    get_v = pltpu.make_async_copy(v_hbm.at[:, pl.ds(kv_at, HD)], kv.at[1, 0], in_sem.at[1])
    get_q = pltpu.make_async_copy(q_hbm, att, in_sem.at[2])
    get_wo = pltpu.make_async_copy(wo_hbm, wo, in_sem.at[3])
    get_tok = [
        pltpu.make_async_copy(
            tok_hbm.at[pl.ds(pl.multiple_of((2 * w + core) * block, 16), block), :],
            apart.at[w, 0, pl.ds(0, block), :],
            t_sem,
        )
        for w in range(n_z)
    ]
    for copy in [get_k, get_v] + get_tok + [get_q, get_wo]:
        copy.start()

    n_grid = n_rows // GRID_W
    for r in range(n_grid):
        for t in range(2):
            trig[t, r * GRID_W : (r + 1) * GRID_W, :] = (
                row_ref[t, pl.ds(ep * n_grid + r, 1), :] + col_ref[t]
            )
    with jax.named_scope("kwait"):
        get_k.wait()
    kv[0, 0] = turned(k_raw[...], kg_ref[...], trig[0], trig[1])
    get_v.wait()
    with jax.named_scope("barrier"):
        pl.semaphore_wait(barrier, n_ep + n_z - 1)
    for s, p in peers[:near]:
        remote(kv.at[core, 0], kv.at[core, back[s]], kv_s, kv_r.at[back[s]], (p, tp)).start()

    with jax.named_scope("gather"):
        def mine(table):
            sides = [
                jnp.concatenate(
                    [table[:, (2 * w + c) * block : (2 * w + c + 1) * block] for w in range(n_z)],
                    axis=1,
                )
                for c in range(2)
            ]
            return jnp.where(core == 0, sides[0], sides[1])

        route = mine(route_ref[...])
        e_iota = lax.broadcasted_iota(jnp.int32, (EXPERTS, half), 0)
        hot0 = (e_iota == route[0:1]).astype(F32)
        hot1 = (e_iota == route[1:2]).astype(F32)
        before = lax.broadcasted_iota(jnp.int32, (half, half), 0)
        after = lax.broadcasted_iota(jnp.int32, (half, half), 1)
        earlier = ((before < after) & (before // block == after // block)).astype(F32)
        count = jnp.dot(
            (hot0 + hot1).astype(BF), earlier.astype(BF), preferred_element_type=F32
        )
        rank0 = jnp.sum(hot0 * count, axis=0, keepdims=True).astype(jnp.int32)
        rank1 = jnp.sum(hot1 * count, axis=0, keepdims=True).astype(jnp.int32)
        base = lax.broadcasted_iota(jnp.int32, (1, half), 1) // block * CAP
        slot0 = route[0:1] * slots + base + rank0
        slot1 = route[1:2] * slots + base + rank1
        j_iota = lax.broadcasted_iota(jnp.int32, (EXPERTS * slots, half), 0)
        is0 = j_iota == slot0
        is1 = j_iota == slot1
        mat = (is0 | is1).astype(F32).astype(BF)
        done(apart.at[:, 0, pl.ds(0, block), :], t_sem)
        get_q.wait()
        get_wo.wait()
        weights = [
            pltpu.make_async_copy(src, dst, w_sem.at[j])
            for j, (src, dst) in enumerate(((wg_hbm, wg), (wu_hbm, wu), (wd_hbm, wd)))
        ]
        for copy in weights:
            copy.start()
        field = apart[:, 0, :block, :].reshape(half, depth).astype(F32)
        normed = (
            field
            * lax.rsqrt(jnp.mean(field * field, axis=-1, keepdims=True) + EPS)
            * ng_ref[...]
        ).astype(BF)
        outb[...] = (
            jnp.dot(mat, normed, preferred_element_type=F32)
            .astype(BF)
            .reshape(n_ep, n_local, slots, depth)
        )
        arr[:, core, 0] = outb[ep]
        remote(outb.at[ep], arr.at[:, core, 0], do_s, do_r, sibling).start()
        share = mine(share_ref[...])
        share = share / jnp.sum(share, axis=0, keepdims=True)
        comb = jnp.where(is0, share[0:1], 0.0) + jnp.where(is1, share[1:2], 0.0)
        high = comb.astype(BF)
        low = (comb - high.astype(F32)).astype(BF)
        both[...] = jnp.concatenate([high, low], axis=1)

    with jax.named_scope("qprep"):
        for g in range(heads):
            qn[pl.ds(g * n_rows, n_rows), :] = turned(
                att[:, g * HD : (g + 1) * HD], qg_ref[...], trig[0], trig[1]
            )

    factor = HD ** (-0.5) * LOG2E

    length = n_ep * n_rows

    def attend(at, g):
        scores = lax.dot_general(
            qn[pl.ds(pl.multiple_of(g * n_rows + at, 16), tile), :],
            kv[0].reshape(length, HD),
            (((1,), (1,)), ((), ())),
            preferred_element_type=F32,
        )
        top = jnp.max(scores, axis=1, keepdims=True)
        weight = jnp.exp2((scores - top) * factor).astype(BF)
        merged = jnp.dot(weight, values[...], preferred_element_type=F32)
        att[pl.ds(at, tile), g * HD : (g + 1) * HD] = (
            merged[:, :HD] / merged[:, HD:]
        ).astype(BF)

    with jax.named_scope("kvw"):
        values[:, HD:] = jnp.ones((length, HD), BF)
        for s, p in peers[:near]:
            with jax.named_scope(f"kv_{s}"):
                done(kv.at[core, s], kv_r.at[s])
            if near < n_ep - 1:
                part_of = pl.ds((s - 1) * n_rows // 2, n_rows // 2)
                remote(
                    kv.at[core, s, part_of],
                    kv.at[core, 3, part_of],
                    kv_s,
                    kv_r.at[3],
                    (peers[2 - s][1], tp),
                ).start()
        for s, p in peers[:near]:
            remote(kv.at[core, s], kv.at[core, s], kvf_s, kvf_r, sibling).start()
        for s, p in peers[near:]:
            with jax.named_scope(f"kv_{s}"):
                done(kv.at[core, s], kv_r.at[s])
            remote(kv.at[core, s], kv.at[core, s], kvf_s, kvf_r, sibling).start()
        for i in range(n_local):
            for s, p in peers:
                remote(
                    outb.at[p, i], arr.at[i, core, back[s]], d_s, d_r.at[i], (p, tp)
                ).start()
        with jax.named_scope('kv_sib'):
            done(kv.at[other, 1:], kvf_r)
        values[:, :HD] = kv[1].reshape(length, HD)

    def pass_on(i):
        done(arr.at[i, core, 1:], d_r.at[i])
        remote(arr.at[i, core, 1:], arr.at[i, core, 1:], df_s, df_r.at[i], sibling).start()

    def right(w):
        return remote(
            asib.at[w], azr.at[0, w], az_s.at[w], az_r.at[0, w], (ep, (z + 1) * 2 + core)
        )

    def left(w):
        return remote(
            asib.at[w], azr.at[1, w], az_s.at[w], az_r.at[1, w], (ep, (z - 1) * 2 + core)
        )

    def hand_over(w):
        done(asib.at[w], a_r.at[w])
        asib[w] = (apart[w, core].astype(F32) + asib[w].astype(F32)).astype(BF)

        @pl.when((z == 0) & (w != 0))
        def _():
            right(w).start()

        @pl.when((z == n_z - 1) & (w != n_z - 1))
        def _():
            left(w).start()

    def relay(t):
        to_right = n_z - 1 - t + z
        to_left = t - (n_z - 1 - z)

        @pl.when((z >= 1) & (z <= t))
        def _():
            copy = right(to_right)
            copy.wait_recv()
            asib[to_right] = (
                asib[to_right].astype(F32) + azr[0, to_right].astype(F32)
            ).astype(BF)
            copy.start()

        @pl.when((z <= n_z - 2) & (n_z - 1 - z <= t))
        def _():
            copy = left(to_left)
            copy.wait_recv()
            asib[to_left] = (
                asib[to_left].astype(F32) + azr[1, to_left].astype(F32)
            ).astype(BF)
            copy.start()

    far = 2 * z // n_z
    order = [(1 - far) * (n_z - 1 - k) + far * k for k in range(n_z)]
    for k, w in enumerate(order):
        if k == n_z - 1:
            with jax.named_scope("pass0"):
                pass_on(0)
        with jax.named_scope("last"):
            for g in range(heads):
                for c in range(pair // tile):
                    attend(pl.multiple_of(w * pair + c * tile, 16), g)
        with jax.named_scope("proj"):
            apart[w] = (
                jnp.dot(
                    att[pl.ds(pl.multiple_of(w * pair, 16), pair), :],
                    wo[...],
                    preferred_element_type=F32,
                )
                .astype(BF)
                .reshape(2, out_rows, depth)
            )
            remote(apart.at[w, other], asib.at[w], a_s, a_r.at[w], sibling).start()
            if k == 0:
                hand_over(w)
            elif k > 1:
                hand_over(order[k - 1])
    with jax.named_scope("hand"):
        hand_over(order[-1])

    n_cut, width = part.shape[0], part.shape[-1]

    def give(i, j):
        done(sib.at[j, i], p_r.at[j, i])
        sib[j, i] = (part[j, i, core].astype(F32) + sib[j, i].astype(F32)).astype(BF)
        for s, p in peers:
            remote(sib.at[j, i, s], ret.at[j, ep, i], r_s, r_r.at[j], (p, tp)).start()
        ret[j, ep, i] = sib[j, i, 0]

    relayed = 1
    if relayed < n_z - 1:
        with jax.named_scope("relay"):
            relay(relayed)
        relayed += 1
    early = 3 * n_cut // 8
    done(arr.at[:, other, 0], do_r)
    for copy in weights:
        copy.wait()
    for i in range(n_local):
        with jax.named_scope(f"disp{i}"):
            done(arr.at[i, other, 1:], df_r.at[i])
            if i + 2 < n_local:
                pass_on(i + 1)
        with jax.named_scope(f"ffn{i}"):
            x = arr[i].reshape(2 * n_ep * slots, depth)
            gate = jnp.dot(x, wg[i], preferred_element_type=F32)
            up = jnp.dot(x, wu[i], preferred_element_type=F32)
            hid[i] = (gate / (1.0 + jnp.exp(-gate)) * up).astype(BF)
            for j in range(0, n_cut, 2):
                down = jnp.dot(
                    hid[i], wd[i, :, j * width : (j + 2) * width], preferred_element_type=F32
                ).astype(BF)
                for c in range(2):
                    part[j + c, i] = down[:, c * width : (c + 1) * width].reshape(
                        2, n_ep, slots, width
                    )
                    remote(
                        part.at[j + c, i, other],
                        sib.at[j + c, i],
                        p_s,
                        p_r.at[j + c, i],
                        sibling,
                    ).start()
        if i + 2 == n_local:
            with jax.named_scope("passl"):
                pass_on(i + 1)
        with jax.named_scope(f"give{i}"):
            for j in range(early):
                give(i, j)
        if i == n_local - 2 and relayed < n_z - 1:
            with jax.named_scope("relay"):
                relay(relayed)
            relayed += 1
    with jax.named_scope("gives"):
        for j in range(early, n_cut):
            for i in range(n_local):
                give(i, j)

    with jax.named_scope("relays"):
        while relayed < n_z - 1:
            relay(relayed)
            relayed += 1

    def settle(j):
        done(ret.at[j, 1:], r_r.at[j])
        rows = lax.dot_general(
            both[...],
            ret[j].reshape(EXPERTS * slots, width),
            (((0,), (0,)), ((), ())),
            preferred_element_type=F32,
        )
        rows = rows[:half] + rows[half:]
        zs[j] = rows.astype(BF).reshape(n_z, block, width)
        for w in z_peers:
            remote(zs.at[j, w], zr.at[j, z], z_s, z_r.at[j], (ep, w * 2 + core)).start()

    def mixed():
        mixed_ref[...] = asib[z]

        @pl.when(z >= 1)
        def _():
            right(z).wait_recv()
            mixed_ref[...] = (mixed_ref[...].astype(F32) + azr[0, z].astype(F32)).astype(BF)

        @pl.when(z <= n_z - 2)
        def _():
            left(z).wait_recv()
            mixed_ref[...] = (mixed_ref[...].astype(F32) + azr[1, z].astype(F32)).astype(BF)

        copy = pltpu.make_async_copy(mixed_ref, mixed_hbm, out_sem.at[0])
        copy.start()

    def expert(j):
        total = zs[j, z].astype(F32)
        done(zr.at[j, 1:], z_r.at[j])
        for w in z_peers:
            total = total + zr[j, w].astype(F32)
        at = pl.ds(j * width, width)
        expert_ref[:, at] = total.astype(BF)
        copy = pltpu.make_async_copy(expert_ref.at[:, at], expert_hbm.at[:, at], out_sem.at[1])
        copy.start()

    for j in range(n_cut):
        with jax.named_scope(f"settle{j}"):
            settle(j)
    with jax.named_scope("mixed"):
        mixed()
    for j in range(n_cut):
        with jax.named_scope(f"expert{j}"):
            expert(j)
    with jax.named_scope("drain"):
        done(kv.at[core, 1:], kv_s)
        done(kv.at[core, 1:], kvf_s)
        done(outb.at[1:], d_s)
        done(outb.at[0], do_s)
        done(arr.at[:, core, 1:], df_s)
        done(asib, a_s)
        done(sib, p_s)
        done(sib.at[:, :, 1:], r_s)
        done(zs.at[:, 1:], z_s)
        for k in range(1, n_z):

            @pl.when(z + k <= n_z - 1)
            def _():
                right(z + k).wait_send()

            @pl.when(z - k >= 0)
            def _():
                left(z - k).wait_send()
    with jax.named_scope("outs"):
        done(mixed_ref, out_sem.at[0])
        done(expert_ref, out_sem.at[1])


def lay_out(mixed_hbm, expert_hbm, mixed_out, expert_out, mixed, expert, sems):
    pairs = ((mixed_hbm, mixed, mixed_out), (expert_hbm, expert, expert_out))
    ins = [pltpu.make_async_copy(a, b, sems.at[0, i]) for i, (a, b, _) in enumerate(pairs)]
    outs = [pltpu.make_async_copy(b, c, sems.at[1, i]) for i, (_, b, c) in enumerate(pairs)]
    for copy in ins:
        copy.start()
    for copy, after in zip(ins, outs):
        copy.wait()
        after.start()
    for copy in outs:
        copy.wait()


def on_device(
    queries,
    keys,
    values,
    query_gain,
    key_gain,
    out_weight,
    tokens_b,
    norm_gain,
    routes,
    route_weight,
    gate_weight,
    up_weight,
    down_weight,
):
    n_ep, n_tp = lax.axis_size("ep"), lax.axis_size("tp")
    n_z = n_tp // 2
    n_rows = queries.shape[0]
    heads = queries.shape[1] // HD
    depth = tokens_b.shape[1]
    local_rows = tokens_b.shape[0]
    block = local_rows // n_tp
    n_local, _, ff = gate_weight.shape
    slots = n_z * CAP
    length = n_rows * n_ep
    n_cut = NCUT
    width = depth // n_cut
    row_table, col_table = tables(length)

    vmem = pl.BlockSpec(memory_space=pltpu.VMEM)
    hbm = pl.BlockSpec(memory_space=pl.ANY)
    dma = pltpu.SemaphoreType.DMA
    out_rows = n_rows // n_tp
    scratch = [
        pltpu.VMEM((out_rows, out_weight.shape[1]), BF),
        pltpu.VMEM((block, depth), BF),
        pltpu.VMEM(out_weight.shape, BF),
        pltpu.VMEM((2, n_rows, HD), F32),
        pltpu.VMEM(gate_weight.shape, BF),
        pltpu.VMEM(up_weight.shape, BF),
        pltpu.VMEM(down_weight.shape, BF),
        pltpu.VMEM((2, n_ep, n_rows, HD), BF),
        pltpu.VMEM((length, 2 * HD), BF),
        pltpu.VMEM((heads * n_rows, HD), BF),
        pltpu.VMEM((n_rows, heads * HD), BF),
        pltpu.VMEM((n_z, 2, out_rows, depth), BF),
        pltpu.VMEM((n_z, out_rows, depth), BF),
        pltpu.VMEM((2, n_z, out_rows, depth), BF),
        pltpu.VMEM((n_ep, n_local, slots, depth), BF),
        pltpu.VMEM((n_local, 2, n_ep, slots, depth), BF),
        pltpu.VMEM((EXPERTS * slots, 2 * n_z * block), BF),
        pltpu.VMEM((n_local, 2 * n_ep * slots, ff), BF),
        pltpu.VMEM((n_cut, n_local, 2, n_ep, slots, width), BF),
        pltpu.VMEM((n_cut, n_local, n_ep, slots, width), BF),
        pltpu.VMEM((n_cut, n_ep, n_local, slots, width), BF),
        pltpu.VMEM((n_cut, n_z, block, width), BF),
        pltpu.VMEM((n_cut, n_z, block, width), BF),
        dma((4,)),
        dma((2,)),
        dma,
        dma((3,)),
        dma,
        dma((n_ep,)),
        dma,
        dma,
        dma,
        dma((n_local,)),
        dma,
        dma((n_local,)),
        dma,
        dma,
        dma,
        dma((n_z,)),
        dma((n_z,)),
        dma((2, n_z)),
        dma,
        dma((n_cut, n_local)),
        dma,
        dma((n_cut,)),
        dma,
        dma((n_cut,)),
    ]
    shapes = (
        jax.ShapeDtypeStruct((out_rows, out_weight.shape[1]), BF),
        jax.ShapeDtypeStruct((block, depth), BF),
    )
    results = pl.pallas_call(
        functools.partial(kernel, n_ep, n_tp),
        out_shape=shapes,
        in_specs=[hbm] * 3 + [vmem] * 4 + [hbm] * 2 + [vmem] * 3 + [hbm] * 3,
        out_specs=(hbm, hbm),
        scratch_shapes=scratch,
        compiler_params=pltpu.CompilerParams(
            collective_id=0, has_side_effects=True, vmem_limit_bytes=67043328
        ),
    )(
        queries,
        keys,
        values,
        jnp.asarray(row_table),
        jnp.asarray(col_table),
        query_gain[None],
        key_gain[None],
        out_weight,
        tokens_b,
        norm_gain[None],
        routes.T,
        route_weight.T,
        gate_weight,
        up_weight,
        down_weight,
    )
    return tuple(
        pl.pallas_call(
            lay_out,
            out_shape=shapes,
            in_specs=[hbm] * 2,
            out_specs=(hbm, hbm),
            scratch_shapes=[pltpu.VMEM(x.shape, BF) for x in shapes] + [dma((2, 2))],
        )(*results)
    )


def solution(mesh):
    placed = (
        P("ep", "tp"),
        P("ep", None),
        P("ep", None),
        P(),
        P(),
        P("tp", None),
        P("ep", None),
        P(),
        P("ep", None),
        P("ep", None),
        P("ep", None, "tp"),
        P("ep", None, "tp"),
        P("ep", "tp", None),
    )
    return jax.shard_map(
        on_device,
        mesh=mesh,
        in_specs=placed,
        out_specs=(P(("ep", "tp"), None), P(("ep", "tp"), None)),
        check_vma=False,
    )
```

time: 92.1 us -> 73.3 us (0.80)
  local copies, waits for them, and re-layouts: 8.08 us -> 0 us
  Pallas kernels: 80.2 us -> 72.3 us
  other arithmetic: 2.83 us -> 0 us
    pallas_call x1 -> x2, Pallas kernels: 80.2 us -> 72.3 us  [the longest x1 70.5 us: on_device(): pl.pallas_call(functools.partial(kernel, n_ep, n_tp), out_shape=shapes, i...]
    unnamed x2 -> x0, local copies, waits for them, and re-layouts: 3.38 us -> none
    reshape x4 -> x0, local copies, waits for them, and re-layouts: 2.88 us -> none  [the longest x2 1.54 us: mine(): split = table.reshape(n_z, 2, block, TOPK)]
    mul x1 -> x0, other arithmetic: 2.8 us -> none  [on_device(): sine = jnp.sin(angle) * jnp.where(lane % (2 * n_freq) < n_freq, -1.0, 1.0)]
    dynamic_slice x3 -> x0, local copies, waits for them, and re-layouts: 1.82 us -> none  [the longest x1 1.79 us: on_device(): own_values = lax.dynamic_slice_in_dim(values, kv_index * HD, HD, 1)]
where the time goes in v1:
time: 73.3 us; the launch traced here: 73.1 us
  Pallas kernels  72.3 us (99%)
  between operations  0.8 us (1%)
    pallas_call x1, Pallas kernels, on_device(): pl.pallas_call(functools.partial(kernel, n_ep, n_tp), out_shape=shapes, i...  70.5 us
    pallas_call x1, Pallas kernels, on_device(): pl.pallas_call(lay_out, out_shape=shapes, in_specs=[hbm] * 2, out_specs=(...  1.84 us

profile of v1, /device:TPU:0, one launch (start us, length us, event | category | flops | bytes accessed | tf_op | source)
XLA Modules:
  0.0 73.1 jit_solution(11892633325471659882)
XLA Ops:
  0.6 70.5 %shard_map.158 = (bf16[96,2048]{1,0:T(8,128)(2,1)}, bf16[48,2048]{1,0:T(8,128)(2,1)}) custom-call(bf16[768,256]{1,0:T(8,128)(2,1)} %q_hbm.1, bf16[768,512]{1,0:T(8,128)(2,1)} %k_hbm.1, bf16[768,512]{1,0:T(8,128)(2,1)} %v_hbm.1, f32[2,48,128]{2,1,0:T(8,128)} %constant.4.clone.row_ref, f32[2,64,128]{2,1,0:T(8,128)} %constant.5.clone.col_ref, ...), custom_call_target="tpu_custom_call" | custom-call | tf_op jit(solution)/shard_map/pallas_call | solution.py:620
  71.1 1.8 %shard_map.159 = (bf16[96,2048]{1,0:T(8,128)(2,1)}, bf16[48,2048]{1,0:T(8,128)(2,1)}) custom-call(bf16[96,2048]{1,0:T(8,128)(2,1)} %get-tuple-element.4.mixed_hbm, bf16[48,2048]{1,0:T(8,128)(2,1)} %get-tuple-element.5.expert_hbm), custom_call_target="tpu_custom_call" | custom-call | tf_op jit(solution)/shard_map/pallas_call | solution.py:647

commit v2 on v1

--- a/solution.py
+++ b/solution.py
@@ -81,8 +81,6 @@
     wg_hbm,
     wu_hbm,
     wd_hbm,
-    mixed_hbm,
-    expert_hbm,
     mixed_ref,
     expert_ref,
     wo,
@@ -107,7 +105,6 @@
     zs,
     zr,
     in_sem,
-    out_sem,
     t_sem,
     w_sem,
     kv_s,
@@ -265,25 +262,52 @@
 
     length = n_ep * n_rows
 
-    def attend(at, g):
+    far = 2 * z // n_z
+    order = [(1 - far) * (n_z - 1 - k) + far * k for k in range(n_z)]
+
+    def scored(at, g, start, end):
         scores = lax.dot_general(
             qn[pl.ds(pl.multiple_of(g * n_rows + at, 16), tile), :],
-            kv[0].reshape(length, HD),
+            kv[0, start:end].reshape((end - start) * n_rows, HD),
             (((1,), (1,)), ((), ())),
             preferred_element_type=F32,
         )
         top = jnp.max(scores, axis=1, keepdims=True)
         weight = jnp.exp2((scores - top) * factor).astype(BF)
-        merged = jnp.dot(weight, values[...], preferred_element_type=F32)
+        return top, jnp.dot(
+            weight, values[start * n_rows : end * n_rows, :], preferred_element_type=F32
+        )
+
+    def attend(at, g, held):
+        if held is None:
+            merged = scored(at, g, 0, n_ep)[1]
+        else:
+            top, merged = scored(at, g, near + 1, n_ep)
+            most = jnp.maximum(top, held[0])
+            merged = merged * jnp.exp2((top - most) * factor) + held[1] * jnp.exp2(
+                (held[0] - most) * factor
+            )
         att[pl.ds(at, tile), g * HD : (g + 1) * HD] = (
             merged[:, :HD] / merged[:, HD:]
         ).astype(BF)
 
+    def tiles(w):
+        return [
+            (pl.multiple_of(w * pair + c * tile, 16), g)
+            for g in range(heads)
+            for c in range(pair // tile)
+        ]
+
+    def fill(start, end):
+        values[start * n_rows : end * n_rows, :HD] = kv[1, start:end].reshape(
+            (end - start) * n_rows, HD
+        )
+
     with jax.named_scope("kvw"):
         values[:, HD:] = jnp.ones((length, HD), BF)
+        fill(0, 1)
         for s, p in peers[:near]:
-            with jax.named_scope(f"kv_{s}"):
-                done(kv.at[core, s], kv_r.at[s])
+            done(kv.at[core, s], kv_r.at[s])
             if near < n_ep - 1:
                 part_of = pl.ds((s - 1) * n_rows // 2, n_rows // 2)
                 remote(
@@ -294,19 +318,25 @@
                     (peers[2 - s][1], tp),
                 ).start()
         for s, p in peers[:near]:
-            remote(kv.at[core, s], kv.at[core, s], kvf_s, kvf_r, sibling).start()
-        for s, p in peers[near:]:
-            with jax.named_scope(f"kv_{s}"):
-                done(kv.at[core, s], kv_r.at[s])
-            remote(kv.at[core, s], kv.at[core, s], kvf_s, kvf_r, sibling).start()
+            remote(kv.at[core, s], kv.at[core, s], kvf_s, kvf_r.at[0], sibling).start()
+        done(kv.at[other, 1 : near + 1], kvf_r.at[0])
+        fill(1, near + 1)
+    first = [None] * len(tiles(0))
+    if near < n_ep - 1:
+        with jax.named_scope("first"):
+            first = [scored(at, g, 0, near + 1) for at, g in tiles(order[0])]
+    with jax.named_scope("kvd"):
         for i in range(n_local):
             for s, p in peers:
                 remote(
                     outb.at[p, i], arr.at[i, core, back[s]], d_s, d_r.at[i], (p, tp)
                 ).start()
-        with jax.named_scope('kv_sib'):
-            done(kv.at[other, 1:], kvf_r)
-        values[:, :HD] = kv[1].reshape(length, HD)
+        if near < n_ep - 1:
+            for s, p in peers[near:]:
+                done(kv.at[core, s], kv_r.at[s])
+                remote(kv.at[core, s], kv.at[core, s], kvf_s, kvf_r.at[1], sibling).start()
+            done(kv.at[other, near + 1 :], kvf_r.at[1])
+            fill(near + 1, n_ep)
 
     def pass_on(i):
         done(arr.at[i, core, 1:], d_r.at[i])
@@ -356,16 +386,13 @@
             ).astype(BF)
             copy.start()
 
-    far = 2 * z // n_z
-    order = [(1 - far) * (n_z - 1 - k) + far * k for k in range(n_z)]
     for k, w in enumerate(order):
         if k == n_z - 1:
             with jax.named_scope("pass0"):
                 pass_on(0)
         with jax.named_scope("last"):
-            for g in range(heads):
-                for c in range(pair // tile):
-                    attend(pl.multiple_of(w * pair + c * tile, 16), g)
+            for (at, g), held in zip(tiles(w), first if k == 0 else [None] * len(first)):
+                attend(at, g, held)
         with jax.named_scope("proj"):
             apart[w] = (
                 jnp.dot(
@@ -473,8 +500,6 @@
             left(z).wait_recv()
             mixed_ref[...] = (mixed_ref[...].astype(F32) + azr[1, z].astype(F32)).astype(BF)
 
-        copy = pltpu.make_async_copy(mixed_ref, mixed_hbm, out_sem.at[0])
-        copy.start()
 
     def expert(j):
         total = zs[j, z].astype(F32)
@@ -483,8 +508,6 @@
             total = total + zr[j, w].astype(F32)
         at = pl.ds(j * width, width)
         expert_ref[:, at] = total.astype(BF)
-        copy = pltpu.make_async_copy(expert_ref.at[:, at], expert_hbm.at[:, at], out_sem.at[1])
-        copy.start()
 
     for j in range(n_cut):
         with jax.named_scope(f"settle{j}"):
@@ -513,22 +536,6 @@
             @pl.when(z - k >= 0)
             def _():
                 left(z - k).wait_send()
-    with jax.named_scope("outs"):
-        done(mixed_ref, out_sem.at[0])
-        done(expert_ref, out_sem.at[1])
-
-
-def lay_out(mixed_hbm, expert_hbm, mixed_out, expert_out, mixed, expert, sems):
-    pairs = ((mixed_hbm, mixed, mixed_out), (expert_hbm, expert, expert_out))
-    ins = [pltpu.make_async_copy(a, b, sems.at[0, i]) for i, (a, b, _) in enumerate(pairs)]
-    outs = [pltpu.make_async_copy(b, c, sems.at[1, i]) for i, (_, b, c) in enumerate(pairs)]
-    for copy in ins:
-        copy.start()
-    for copy, after in zip(ins, outs):
-        copy.wait()
-        after.start()
-    for copy in outs:
-        copy.wait()
 
 
 def on_device(
@@ -565,8 +572,6 @@
     dma = pltpu.SemaphoreType.DMA
     out_rows = n_rows // n_tp
     scratch = [
-        pltpu.VMEM((out_rows, out_weight.shape[1]), BF),
-        pltpu.VMEM((block, depth), BF),
         pltpu.VMEM(out_weight.shape, BF),
         pltpu.VMEM((2, n_rows, HD), F32),
         pltpu.VMEM(gate_weight.shape, BF),
@@ -589,13 +594,12 @@
         pltpu.VMEM((n_cut, n_z, block, width), BF),
         pltpu.VMEM((n_cut, n_z, block, width), BF),
         dma((4,)),
+        dma,
+        dma((3,)),
+        dma,
+        dma((n_ep,)),
+        dma,
         dma((2,)),
-        dma,
-        dma((3,)),
-        dma,
-        dma((n_ep,)),
-        dma,
-        dma,
         dma,
         dma((n_local,)),
         dma,
@@ -613,18 +617,19 @@
         dma,
         dma((n_cut,)),
     ]
+    out_bytes = 2 * (out_rows + block) * depth + 2**17
     shapes = (
         jax.ShapeDtypeStruct((out_rows, out_weight.shape[1]), BF),
         jax.ShapeDtypeStruct((block, depth), BF),
     )
     results = pl.pallas_call(
         functools.partial(kernel, n_ep, n_tp),
-        out_shape=shapes,
+        out_shape=tuple(pltpu.VMEM(x.shape, x.dtype) for x in shapes),
         in_specs=[hbm] * 3 + [vmem] * 4 + [hbm] * 2 + [vmem] * 3 + [hbm] * 3,
-        out_specs=(hbm, hbm),
+        out_specs=(vmem, vmem),
         scratch_shapes=scratch,
         compiler_params=pltpu.CompilerParams(
-            collective_id=0, has_side_effects=True, vmem_limit_bytes=67043328
+            collective_id=0, has_side_effects=True, vmem_limit_bytes=67043328 - out_bytes
         ),
     )(
         queries,
@@ -643,15 +648,7 @@
         up_weight,
         down_weight,
     )
-    return tuple(
-        pl.pallas_call(
-            lay_out,
-            out_shape=shapes,
-            in_specs=[hbm] * 2,
-            out_specs=(hbm, hbm),
-            scratch_shapes=[pltpu.VMEM(x.shape, BF) for x in shapes] + [dma((2, 2))],
-        )(*results)
-    )
+    return tuple(results)
 
 
 def solution(mesh):

time: 73.3 us -> 70.7 us (0.965)
  Pallas kernels: 72.3 us -> 68.5 us
  local copies, waits for them, and re-layouts: 0 us -> 1.42 us
    pallas_call x2 -> x1, Pallas kernels: 72.3 us -> 68.5 us  [on_device(): pl.pallas_call(functools.partial(kernel, n_ep, n_tp), out_shape=tuple((pl...]
    unnamed x0 -> x2, local copies, waits for them, and re-layouts: none -> 1.42 us
where the time goes in v2:
time: 70.7 us; the launch traced here: 70.5 us
  Pallas kernels  68.5 us (97%)
  local copies, waits for them, and re-layouts  1.42 us (2%)
    pallas_call x1, Pallas kernels, on_device(): pl.pallas_call(functools.partial(kernel, n_ep, n_tp), out_shape=tuple((pl...  68.5 us
    unnamed x2, local copies, waits for them, and re-layouts  1.42 us

profile of v2, /device:TPU:0, one launch (start us, length us, event | category | flops | bytes accessed | tf_op | source)
XLA Modules:
  0.0 70.5 jit_solution(6396757782151332399)
XLA Ops:
  0.6 68.5 %shard_map.158 = (bf16[96,2048]{1,0:T(8,128)(2,1)S(1)}, bf16[48,2048]{1,0:T(8,128)(2,1)S(1)}) custom-call(bf16[768,256]{1,0:T(8,128)(2,1)} %q_hbm.1, bf16[768,512]{1,0:T(8,128)(2,1)} %k_hbm.1, bf16[768,512]{1,0:T(8,128)(2,1)} %v_hbm.1, f32[2,48,128]{2,1,0:T(8,128)} %constant.4.clone.row_ref, f32[2,64,128]{2,1,0:T(8,128)} %constant.5.clone.col_ref, ...), custom_call_target="tpu_custom_call" | custom-call | tf_op jit(solution)/shard_map/pallas_call | solution.py:625
  69.1 0.7 %copy.19 = bf16[96,2048]{1,0:T(8,128)(2,1)} copy(bf16[96,2048]{1,0:T(8,128)(2,1)S(1)} %get-tuple-element.2) | data formatting | bytes 786432
  69.8 0.7 copy.20
